TPU v7x, 32 devices: a whole 2x2x4 slice. The times are simulated.
32 devices in a mesh: sp: 16 (over z, y, x), tp: 2 (over core).
Axes of the slice: x: 2, y: 2, z: 4, core: 2. Of those that a mesh axis runs over, the one named last changes fastest.
Arguments:
- tokens: bfloat16 [4096, 2048], P(('sp', 'tp')), may hold values from -6 to 6
- gain: float32 [2048], replicated, may hold values from 0.1 to 1.9
- w_ret_q: bfloat16 [2048, 2048], P(None, 'tp'), may hold values from -0.125 to 0.125
- w_ret_k: bfloat16 [2048, 2048], P(None, 'tp'), may hold values from -0.125 to 0.125
- w_ret_v: bfloat16 [2048, 2048], P(None, 'tp'), may hold values from -0.125 to 0.125
- w_fox_q: bfloat16 [2048, 1024], P(None, 'tp'), may hold values from -0.125 to 0.125
- w_fox_k: bfloat16 [2048, 1024], P(None, 'tp'), may hold values from -0.125 to 0.125
- w_fox_v: bfloat16 [2048, 1024], P(None, 'tp'), may hold values from -0.125 to 0.125
- fox_gates: float32 [4096, 8], P('sp', 'tp'), may hold values from -4096 to 0, as said below
- w_out_ret: bfloat16 [2048, 2048], P('tp', 'sp'), may hold values from -0.109375 to 0.109375
- w_out_fox: bfloat16 [1024, 2048], P('tp', 'sp'), may hold values from -0.109375 to 0.109375
Outputs:
- mixed: bfloat16 [4096, 2048], P(('sp', 'tp'))
Inputs may be any that keep to these rules, and one draw needn't show every extreme that they name: `fox_gates`: each head's values never rise along positions.
All inputs are finite; a program needn't handle non-finite values.
Results may differ from a plain program's by a relative error of at most 0.02.
Values may be sent and summed in bfloat16 or wider, within the bound.
A program may use at most 128 MiB of HBM per device.

v0:
```python
import math

import jax
import jax.numpy as jnp
from jax import lax
from jax.sharding import PartitionSpec as P

RET_HEADS = 8
RET_DIM = 256
FOX_DIM = 128
BLOCK = 128


eps = 1e-06


def prefix(part, axis, combine, identity):
    place = lax.axis_index(axis)
    gathered = jax.tree.map(lambda a: lax.all_gather(a, axis), part)
    state = jax.tree.map(lambda a, e: jnp.zeros_like(a) + jnp.asarray(e, a.dtype), part, identity)

    def one(lap, state):
        return combine(
            state, jax.tree.map(lambda a: lax.dynamic_index_in_dim(a, lap, 0, False), gathered)
        )

    return lax.fori_loop(0, place, one, state)


def head_norm(values, width):
    rows_here = values.shape[0]
    grouped = values.reshape(rows_here, -1, width)
    scaled = grouped * lax.rsqrt(jnp.mean(grouped * grouped, axis=2, keepdims=True) + eps)
    return scaled.reshape(rows_here, -1).astype(jnp.bfloat16)


def rotate(values, token_positions, width):
    rows_here = values.shape[0]
    half_width = width // 2
    inverse = 10000.0 ** (-jnp.arange(half_width, dtype=jnp.float32) / half_width)
    angles = token_positions.astype(jnp.float32)[:, None] * inverse[None, :]
    cosine = jnp.cos(angles)[:, None, :]
    sine = jnp.sin(angles)[:, None, :]
    grouped = values.astype(jnp.float32).reshape(rows_here, -1, width)
    first_half = grouped[..., :half_width]
    second_half = grouped[..., half_width:]
    turned = jnp.concatenate(
        [first_half * cosine - second_half * sine, first_half * sine + second_half * cosine],
        axis=-1,
    )
    return turned.reshape(rows_here, -1)


def decay_rates(head_ids, total):
    heads_float = head_ids.astype(jnp.float32)
    middle = RET_HEADS // 2
    fast_rate = 1.0 / (32.0 + 16.0 * heads_float)
    slow_rate = jnp.exp2(-(heads_float - middle)) / total
    return jnp.where(head_ids < middle, fast_rate, slow_rate)


def decay_tables(rates):
    offsets = jnp.arange(BLOCK, dtype=jnp.float32)
    spread = offsets[:, None] - offsets[None, :]
    causal = spread >= 0
    within = jnp.where(
        causal[None], jnp.exp(-rates[:, None, None] * jnp.where(causal, spread, 0.0)[None]), 0.0
    )
    query_decay = jnp.exp(-rates[None, :] * (offsets[:, None] + 1.0))
    key_decay = jnp.exp(-rates[None, :] * (BLOCK - 1.0 - offsets[:, None]))
    block_decay = jnp.exp(-rates * BLOCK)
    return (within, query_decay, key_decay, block_decay)


def advance(carry, key_block, value_block, key_decay, block_decay):
    scaled = (key_block.astype(jnp.float32) * key_decay[:, :, None]).astype(jnp.bfloat16)
    update = jnp.einsum("shd,she->hde", scaled, value_block, preferred_element_type=jnp.float32)
    return carry * block_decay[:, None, None] + update


def retention_blocks(queries, keys, values, rates, state, heads):
    within, query_decay, key_decay, block_decay = decay_tables(rates)
    count = queries.shape[0] // BLOCK

    def shaped(array):
        return array.reshape(count, BLOCK, heads, RET_DIM)

    def retention_step(carry, blocks):
        query_block, key_block, value_block = blocks
        scores = (
            jnp.einsum("thd,shd->hts", query_block, key_block, preferred_element_type=jnp.float32)
            * within
        )
        inner = jnp.einsum(
            "hts,she->the",
            scores.astype(jnp.bfloat16),
            value_block,
            preferred_element_type=jnp.float32,
        )
        cross = (
            jnp.einsum(
                "thd,hde->the",
                query_block.astype(jnp.float32),
                carry,
                precision=lax.Precision.HIGHEST,
            )
            * query_decay[:, :, None]
        )
        return (advance(carry, key_block, value_block, key_decay, block_decay), inner + cross)

    final_state, outputs = lax.scan(
        retention_step, state, (shaped(queries), shaped(keys), shaped(values))
    )
    return (final_state, outputs.reshape(count * BLOCK, heads * RET_DIM))


def block_states(keys, values, rates, heads):
    _, _, key_decay, block_decay = decay_tables(rates)
    count = keys.shape[0] // BLOCK

    def block_step(carry, blocks):
        return (advance(carry, blocks[0], blocks[1], key_decay, block_decay), None)

    start_state = jnp.zeros((heads, RET_DIM, RET_DIM), jnp.float32)
    blocks = (
        keys.reshape(count, BLOCK, heads, RET_DIM),
        values.reshape(count, BLOCK, heads, RET_DIM),
    )
    final_state, _ = lax.scan(block_step, start_state, blocks)
    return final_state


def join_states(earlier, later):
    return (earlier[0] * later[0], earlier[1] * later[0][:, None, None] + later[1])


def fox_weights(queries, keys, query_gates, key_gates, query_pos, key_pos):
    scores = jnp.einsum(
        "qhd,khd->hqk", queries, keys, preferred_element_type=jnp.float32
    ) * FOX_DIM ** (-0.5)
    scores = scores + query_gates.T[:, :, None] - key_gates.T[:, None, :]
    allowed = key_pos[None, :] <= query_pos[:, None]
    return jnp.exp(jnp.where(allowed[None], scores, -jnp.inf))


def add_block(numer, denom, weights, values):
    numer = numer + jnp.einsum(
        "hqk,khd->qhd", weights.astype(jnp.bfloat16), values, preferred_element_type=jnp.float32
    )
    denom = denom + jnp.sum(weights, axis=2).T
    return (numer, denom)


def per_device(
    tokens,
    gain,
    w_ret_q,
    w_ret_k,
    w_ret_v,
    w_fox_q,
    w_fox_k,
    w_fox_v,
    fox_gates,
    w_out_ret,
    w_out_fox,
):
    inputs = tokens.astype(jnp.float32)
    normed = (
        inputs * lax.rsqrt(jnp.mean(inputs * inputs, axis=1, keepdims=True) + eps) * gain
    ).astype(jnp.bfloat16)
    weights_in = (w_ret_q, w_ret_k, w_ret_v, w_fox_q, w_fox_k, w_fox_v)
    piece = lax.all_gather(normed, "tp", axis=0, tiled=True)
    products = [jnp.dot(piece, matrix, preferred_element_type=jnp.float32) for matrix in weights_in]
    projected = jnp.concatenate(products, axis=1).astype(jnp.bfloat16)
    ret_width = w_ret_q.shape[1]
    fox_width = w_fox_q.shape[1]
    edges = [
        0,
        ret_width,
        2 * ret_width,
        3 * ret_width,
        3 * ret_width + fox_width,
        3 * ret_width + 2 * fox_width,
        3 * ret_width + 3 * fox_width,
    ]
    pieces_out = [projected[:, edges[column] : edges[column + 1]] for column in range(6)]
    ret_query, ret_key, ret_value, fox_query, fox_key, fox_value = pieces_out
    length = projected.shape[0]
    sp_count = lax.axis_size("sp")
    total = length * sp_count
    offset = lax.axis_index("sp") * length
    token_positions = offset + jnp.arange(length, dtype=jnp.int32)
    ret_heads = ret_width // RET_DIM
    fox_heads = fox_width // FOX_DIM
    head_ids = lax.axis_index("tp") * ret_heads + jnp.arange(ret_heads, dtype=jnp.int32)
    rates = decay_rates(head_ids, float(total))
    query_rot = rotate(ret_query, token_positions, RET_DIM).astype(jnp.bfloat16)
    key_rot = (rotate(ret_key, token_positions, RET_DIM) * RET_DIM ** (-0.5)).astype(jnp.bfloat16)
    span_decay = jnp.exp(-rates * length)
    empty_state = jnp.zeros((ret_heads, RET_DIM, RET_DIM), jnp.float32)
    identity = (jnp.ones_like(span_decay), empty_state)
    final_state = block_states(key_rot, ret_value, rates, ret_heads)
    carried = prefix((span_decay, final_state), "sp", join_states, identity)[1]
    ret_raw = retention_blocks(query_rot, key_rot, ret_value, rates, carried, ret_heads)[1]
    ret_mixed = head_norm(ret_raw, RET_DIM)
    gates_all = lax.all_gather(fox_gates, "sp", axis=0, tiled=True)
    query3 = fox_query.reshape(length, fox_heads, FOX_DIM)
    zero_numer = jnp.zeros((length, fox_heads, FOX_DIM), jnp.float32)
    zero_denom = jnp.zeros((length, fox_heads), jnp.float32)
    last_query = offset + length - 1
    keys = lax.all_gather(fox_key, "sp", axis=0, tiled=True)
    values = lax.all_gather(fox_value, "sp", axis=0, tiled=True)
    rows_here = keys.shape[0]
    width = math.gcd(rows_here, 512)

    def one_block(state, index):
        begin = index * width

        def compute(accum):
            key_block = lax.dynamic_slice_in_dim(keys, begin, width, 0).reshape(
                width, fox_heads, FOX_DIM
            )
            value_block = lax.dynamic_slice_in_dim(values, begin, width, 0).reshape(
                width, fox_heads, FOX_DIM
            )
            key_gates = lax.dynamic_slice_in_dim(gates_all, begin, width, 0)
            key_pos = begin + jnp.arange(width, dtype=jnp.int32)
            weights = fox_weights(query3, key_block, fox_gates, key_gates, token_positions, key_pos)
            return add_block(accum[0], accum[1], weights, value_block)

        def skip(accum):
            return accum

        return (lax.cond(begin <= last_query, compute, skip, state), None)

    result, _ = lax.scan(
        one_block, (zero_numer, zero_denom), jnp.arange(rows_here // width, dtype=jnp.int32)
    )
    numer, denom = result
    fox_raw = (numer / denom[:, :, None]).reshape(length, fox_width)
    fox_mixed = head_norm(fox_raw, FOX_DIM)
    out_ret, out_fox = (
        lax.all_gather(w_out_ret, "sp", axis=1, tiled=True),
        lax.all_gather(w_out_fox, "sp", axis=1, tiled=True),
    )
    return lax.psum_scatter(
        (
            jnp.dot(ret_mixed, out_ret, preferred_element_type=jnp.float32)
            + jnp.dot(fox_mixed, out_fox, preferred_element_type=jnp.float32)
        ).astype(jnp.bfloat16),
        "tp",
        scatter_dimension=0,
        tiled=True,
    )


def solution(mesh):
    in_specs = (
        P(("sp", "tp"), None),
        P(),
        P(None, "tp"),
        P(None, "tp"),
        P(None, "tp"),
        P(None, "tp"),
        P(None, "tp"),
        P(None, "tp"),
        P("sp", "tp"),
        P("tp", "sp"),
        P("tp", "sp"),
    )
    out_specs = P(("sp", "tp"), None)
    return jax.shard_map(
        per_device, mesh=mesh, in_specs=in_specs, out_specs=out_specs, check_vma=False
    )
```

profile of v0, /device:TPU:0, one launch (start us, length us, event | category | flops | bytes accessed | tf_op | source)
XLA Modules:
  0.0 542.5 jit_solution(13365814762456692468)
XLA Ops:
  7.9 2.0 fusion.64
  10.0 11.9 %all-gather.9.cloned.1.call-done = bf16[256,2048]{1,0:T(8,128)(2,1)} async-done(((bf16[128,2048]{1,0:T(8,128)(2,1)}), bf16[256,2048]{1,0:T(8,128)(2,1)}) %all-gather.9.cloned.1.call-update) | async-done | bytes 1048592 | tf_op jit(solution)/shard_map/all_gather | solution.py:172
  21.9 2.7 convolution_convert_fusion.5
  24.7 3.0 convolution_convert_fusion.4
  28.4 3.4 fusion.60
  32.3 3.9 fusion.59
  37.8 3.8 convolution_convert_fusion.1
  47.6 41.5 %all-gather.1 = f32[16,1,4]{2,1,0:T(1,128)S(1)} all-gather(f32[1,1,4]{2,1,0:T(1,128)S(1)} %exponential_bitcast_fusion), channel_id=1, replica_groups=mesh['sp'=16,'tp'=2] {'sp'}, dimensions={0}, use_global_device_ids=true | all-gather | bytes 272 | tf_op jit(solution)/shard_map/all_gather | solution.py:19
  89.1 36.1 %all_gather.35 = f32[4096,4]{0,1:T(4,128)S(1)} all-gather(f32[256,4]{0,1:T(4,128)S(1)} %copy-done.4), channel_id=1, replica_groups=mesh['sp'=16,'tp'=2] {'sp'}, dimensions={0}, use_global_device_ids=true | all-gather | bytes 69632 | tf_op jit(solution)/shard_map/all_gather | solution.py:206
  125.2 2.6 fusion.61
  128.0 6.5 %copy.78 = bf16[4096,512]{0,1:T(8,128)(2,1)} copy(bf16[4096,512]{1,0:T(8,128)(2,1)} %all-gather.13.cloned.1.call-done) | data formatting | bytes 8388608
  134.5 44.9 %all-gather.15.cloned.1.call-done = bf16[4096,512]{1,0:T(8,128)(2,1)} async-done(((bf16[256,512]{1,0:T(8,128)(2,1)}), bf16[4096,512]{1,0:T(8,128)(2,1)}) %all-gather.15.cloned.1.call-update) | async-done | bytes 4194320 | tf_op jit(solution)/shard_map/all_gather | solution.py:211
  179.4 6.4 %copy.79 = bf16[4096,512]{0,1:T(8,128)(2,1)} copy(bf16[4096,512]{1,0:T(8,128)(2,1)} %all-gather.15.cloned.1.call-done) | data formatting | bytes 8388608
  185.8 13.7 %while.51 = (s32[]{:T(128)}, f32[256,4,128]{0,2,1:T(8,128)S(1)}, f32[256,4]{0,1:T(4,128)S(1)}, s32[8]{0:T(128)S(1)}, s32[]{:T(128)}, /*index=5*/bf16[4096,512]{0...) while((s32[]{:T(128)}, f32[256,4,128]{0,2,1:T(8,128)S(1)}, ...), condition=%wide.region_12.13_spmd.clone, body=%wide.region_8.12_spmd.clone.sunk | while | flops 271844096 | bytes 6869325 | solution.py:236
  187.1 3.4 conditional.3
  187.1 1.9 constant_dynamic-slice_fusion
  199.7 171.9 %all-gather.19.cloned.1.call-done = f32[64,256,256]{2,1,0:T(8,128)} async-done(((f32[4,256,256]{2,1,0:T(8,128)}), f32[64,256,256]{2,1,0:T(8,128)}) %all-gather.19.cloned.1.call-update) | async-done | bytes 16777232 | tf_op jit(solution)/shard_map/all_gather | solution.py:19
  371.9 6.1 %while.53 = (s32[]{:T(128)}, f32[4,256,256]{2,1,0:T(8,128)S(1)}, f32[2,128,4,256]{1,3,2,0:T(8,128)}, bf16[2,128,4,256]{3,1,0,2:T(8,128)(2,1)S(1)}, bf16[2,128,4,...) while((s32[]{:T(128)}, f32[4,256,256]{2,1,0:T(8,128)S(1)}, ...), condition=%wide.region_6.7_spmd.clone.clone, body=%wide.region_5.6_spmd.clone.clone.sunk | while | flops 538313792 | bytes 6387361 | solution.py:111
  372.4 1.9 fusion.110
  380.7 80.4 %all-gather.11.cloned.1.call-done = bf16[1024,2048]{1,0:T(8,128)(2,1)} async-done(((bf16[1024,128]{1,0:T(8,128)(2,1)}), bf16[1024,2048]{1,0:T(8,128)(2,1)}) %all-gather.11.cloned.1.call-update) | async-done | bytes 4194320 | tf_op jit(solution)/shard_map/all_gather | solution.py:243
  461.1 4.8 fusion.66
  465.9 58.9 %all-gather.17.cloned.1.call-done = bf16[512,2048]{1,0:T(8,128)(2,1)} async-done(((bf16[512,128]{1,0:T(8,128)(2,1)}), bf16[512,2048]{1,0:T(8,128)(2,1)}) %all-gather.17.cloned.1.call-update) | async-done | bytes 2097168 | tf_op jit(solution)/shard_map/all_gather | solution.py:244
  524.8 4.1 fusion.58
  528.9 6.7 %reduce-scatter.2.cloned.1.call-done = bf16[128,2048]{1,0:T(8,128)(2,1)} async-done(((bf16[256,2048]{1,0:T(8,128)(2,1)}), bf16[128,2048]{1,0:T(8,128)(2,1)}) %reduce-scatter.2.cloned.1.call-update) | async-done | bytes 524304 | tf_op jit(solution)/shard_map/reduce_scatter | solution.py:246
  (113 shorter events, 25.1 us)
Async XLA Ops:
  6.5 15.4 %copy-start = (bf16[2048,512]{1,0:T(8,128)(2,1)S(1)}, bf16[2048,512]{1,0:T(8,128)(2,1)}, u32[]{:S(2)}) copy-start(bf16[2048,512]{1,0:T(8,128)(2,1)} %param.28) | copy-start | bytes 6291460
  6.5 15.3 %all-gather.9.cloned.1.call-start = ((), (), s32[]{:S(2)}) async-start(), calls=%async_computation.1 | async-start | bytes 1572864 | tf_op jit(solution)/shard_map/all_gather | solution.py:172
  10.0 118.0 %all-gather.13.cloned.1.call-start = ((), (), s32[]{:S(2)}) async-start(), calls=%async_computation.3 | async-start | bytes 4456448 | tf_op jit(solution)/shard_map/all_gather | solution.py:212
  21.9 2.8 copy-start.5
  24.6 154.7 %all-gather.15.cloned.1.call-start = ((), (), s32[]{:S(2)}) async-start(), calls=%async_computation.4 | async-start | bytes 4456448 | tf_op jit(solution)/shard_map/all_gather | solution.py:211
  27.7 343.9 %all-gather.19.cloned.1.call-start = ((), (), s32[]{:S(2)}) async-start(), calls=%async_computation.7 | async-start | bytes 17825792 | tf_op jit(solution)/shard_map/all_gather | solution.py:19
  43.8 45.3 %copy-start.4 = (f32[256,4]{0,1:T(4,128)S(1)}, f32[256,4]{0,1:T(4,128)}, u32[]{:S(2)}) copy-start(f32[256,4]{0,1:T(4,128)} %param.29) | copy-start | bytes 12292
  45.2 1.0 copy-start.2
  46.3 414.9 %all-gather.11.cloned.1.call-start = ((), (), s32[]{:S(2)}) async-start(), calls=%async_computation.2 | async-start | bytes 4456448 | tf_op jit(solution)/shard_map/all_gather | solution.py:243
  46.9 478.0 %all-gather.17.cloned.1.call-start = ((), (), s32[]{:S(2)}) async-start(), calls=%async_computation.5 | async-start | bytes 2228224 | tf_op jit(solution)/shard_map/all_gather | solution.py:244
  47.4 488.2 %reduce-scatter.2.cloned.1.call-start = ((), (), s32[]{:S(2)}) async-start(), calls=%async_computation.6 | async-start | bytes 1572864 | tf_op jit(solution)/shard_map/reduce_scatter | solution.py:246
  378.0 1.7 copy-start.3
  524.8 10.8 %copy-start.1 = (bf16[2048,512]{1,0:T(8,128)(2,1)S(1)}, bf16[2048,512]{1,0:T(8,128)(2,1)}, u32[]{:S(2)}) copy-start(bf16[2048,512]{1,0:T(8,128)(2,1)} %param.28) | copy-start | bytes 6291460
Sparse Core Ops, SparseCore 0:
  10.1 11.7 all-gather.8
  24.8 77.4 all-gather.12
  105.0 74.3 all-gather.14
  182.0 189.5 all-gather.18
  374.2 86.8 all-gather.10
  463.7 61.1 all-gather.16
  529.0 6.5 reduce-scatter.1
where the time goes:
time: 544 us; the launch traced here: 543 us
  waiting for transfers between devices  376 us (69%)
  blocking collectives  77.7 us (14%)
  matrix products  36.2 us (7%)
  local copies, waits for them, and re-layouts  27.5 us (5%)
  between operations  13.8 us (3%)
  loops' own time  5.99 us (1%)
    all_gather x1, waiting for transfers between devices, prefix(): gathered = jax.tree.map(lambda a: lax.all_gather(a, axis), part)  172 us
    all_gather x1, waiting for transfers between devices, per_device(): lax.all_gather(w_out_ret, 'sp', axis=1, tiled=True)  80.4 us
    all_gather x1, waiting for transfers between devices, per_device(): lax.all_gather(w_out_fox, 'sp', axis=1, tiled=True)  58.9 us
    all_gather x1, waiting for transfers between devices, per_device(): keys = lax.all_gather(fox_key, 'sp', axis=0, tiled=True)  44.9 us
    all_gather x1, blocking collectives, prefix(): gathered = jax.tree.map(lambda a: lax.all_gather(a, axis), part)  41.5 us
    all_gather x1, blocking collectives, per_device(): gates_all = lax.all_gather(fox_gates, 'sp', axis=0, tiled=True)  36.1 us
    dot_general x6, matrix products, per_device(): jnp.dot(piece, matrix, preferred_element_type=jnp.float32)  19.5 us
    unnamed x17, local copies, waits for them, and re-layouts  14.3 us
  transfers between devices with their start and end apart: 7, of which 6 were waited for; matrix products, arithmetic and copies ran while one was open for 11% of the time, Pallas kernels for 0%

commit v1 on v0

v1 whole, which is shorter than its diff:
```python
import functools
import math

import jax
import jax.numpy as jnp
from jax import lax
from jax.experimental import pallas as pl
from jax.experimental.pallas import tpu as pltpu
from jax.sharding import PartitionSpec as P

RET_HEADS = 8
RET_DIM = 256
FOX_DIM = 128
BLOCK = 128
MESH = pl.DeviceIdType.MESH
VMEM_LIMIT = 60 * 1024 * 1024

eps = 1e-06


def remote(src, dst, send, recv, sp, tp):
    return pltpu.make_async_remote_copy(
        src_ref=src,
        dst_ref=dst,
        send_sem=send,
        recv_sem=recv,
        device_id=(sp, tp),
        device_id_type=MESH,
    )


def gather_kernel(
    n_sp,
    n_tp,
    group,
    tok_ref,
    gain_ref,
    gates_ref,
    wr_ref,
    wf_ref,
    xall,
    gall,
    wz,
    own,
    local_sem,
    tsend,
    trecv,
    dsend,
    drecv,
    psend,
    precv,
    gsend,
    grecv,
    usend,
    urecv,
    nsend,
    nrecv,
):
    sp = lax.axis_index("sp")
    tp = lax.axis_index("tp")
    g = lax.rem(sp, group)
    z = sp // group
    depth = n_sp // group
    rows = tok_ref.shape[0]
    half = rows // 2
    krows = wr_ref.shape[0]

    barrier = pltpu.get_barrier_semaphore()
    for i in range(1, n_sp):
        pl.semaphore_signal(
            barrier, inc=1, device_id=(lax.rem(sp + i, n_sp), tp), device_id_type=MESH
        )
    for i in range(1, n_tp):
        pl.semaphore_signal(
            barrier, inc=1, device_id=(sp, lax.rem(tp + i, n_tp)), device_id_type=MESH
        )

    values = tok_ref[...].astype(jnp.float32)
    scale = lax.rsqrt(jnp.mean(values * values, axis=1, keepdims=True) + eps)
    own[...] = (values * scale * gain_ref[...]).astype(jnp.bfloat16)
    copies = [
        pltpu.make_async_copy(wr_ref, wz.at[z, pl.ds(0, krows)], local_sem.at[0]),
        pltpu.make_async_copy(
            wf_ref, wz.at[z, pl.ds(krows, wf_ref.shape[0])], local_sem.at[1]
        ),
        pltpu.make_async_copy(gates_ref, gall.at[sp], local_sem.at[2]),
    ]
    for copy in copies:
        copy.start()
    pl.semaphore_wait(barrier, n_sp + n_tp - 2)

    def slot(which, core):
        return xall.at[which * n_tp + core]

    mine = pltpu.make_async_copy(own, slot(g, tp), local_sem.at[3])
    mine.start()

    def peer(other):
        return z * group + other

    hyper = group == 4
    direct = []
    for i in range(1, group):
        if hyper and i == 3:
            continue
        other = lax.bitwise_xor(g, i) if hyper else lax.rem(g + i, group)
        direct.append(
            remote(own, slot(g, tp), tsend.at[i], trecv.at[i], peer(other), tp)
        )
    for copy in direct:
        copy.start()
    pair = []
    for i in range(1, n_tp):
        copy = remote(
            own, slot(g, tp), psend.at[0, i], precv.at[0, i], sp, lax.rem(tp + i, n_tp)
        )
        copy.start()
        pair.append(copy)
    gate_copies = []
    for i in range(1, n_sp):
        copy = remote(
            gates_ref, gall.at[sp], gsend.at[i], grecv.at[i], lax.rem(sp + i, n_sp), tp
        )
        copy.start()
        gate_copies.append(copy)

    copies[0].wait()
    copies[1].wait()

    def up(block):
        return remote(
            wz.at[block],
            wz.at[block],
            usend.at[block],
            urecv.at[block],
            lax.rem(sp + group, n_sp),
            tp,
        )

    def down(block):
        return remote(
            wz.at[block],
            wz.at[block],
            nsend.at[block],
            nrecv.at[block],
            lax.rem(sp + n_sp - group, n_sp),
            tp,
        )

    @pl.when(z < depth - 1)
    def _():
        up(z).start()

    @pl.when(z > 0)
    def _():
        down(z).start()

    def forward(which, row):
        for i in range(1, n_tp):
            copy = remote(
                slot(which, tp),
                slot(which, tp),
                psend.at[row, i],
                precv.at[row, i],
                sp,
                lax.rem(tp + i, n_tp),
            )
            copy.start()
            pair.append(copy)

    if hyper:
        relays = []
        for i in (1, 2):
            direct[i - 1].wait_recv()
            source = lax.bitwise_xor(g, i)
            target = lax.bitwise_xor(g, 3 - i)
            part = pl.ds((i - 1) * half, half)
            copy = remote(
                slot(source, tp).at[part],
                slot(source, tp).at[part],
                dsend.at[i],
                drecv.at[i],
                peer(target),
                tp,
            )
            copy.start()
            relays.append(copy)
            forward(source, i)
    else:
        for i in range(1, group):
            direct[i - 1].wait_recv()
            forward(lax.rem(g + group - i, group), i)

    def line(step, carry):
        below = z - step
        above = z + step

        @pl.when(below >= 0)
        def _():
            up(below).wait_recv()

            @pl.when(z < depth - 1)
            def _():
                up(below).start()

        @pl.when(above <= depth - 1)
        def _():
            down(above).wait_recv()

            @pl.when(z > 0)
            def _():
                down(above).start()

        return carry

    split = depth // 2 if hyper else depth
    lax.fori_loop(1, split, line, 0)
    if hyper:
        for copy in relays:
            copy.wait_recv()
        forward(lax.bitwise_xor(g, 3), 3)
    lax.fori_loop(split, depth, line, 0)

    def settle(step, carry):
        @pl.when((z < depth - 1) & (step <= z))
        def _():
            up(step).wait_send()

        @pl.when((z > 0) & (step >= z))
        def _():
            down(step).wait_send()

        return carry

    lax.fori_loop(0, depth, settle, 0)
    for copy in direct:
        copy.wait_send()
    if hyper:
        for copy in relays:
            copy.wait_send()
    for copy in gate_copies + pair:
        copy.wait()
    copies[2].wait()
    mine.wait()


def gather(tokens, gain, gates, w_ret, w_fox, n_sp, n_tp, group):
    rows, width = tokens.shape
    depth = n_sp // group
    out_rows = w_ret.shape[0] + w_fox.shape[0]
    vmem = pl.BlockSpec(memory_space=pltpu.VMEM)
    hbm = pl.BlockSpec(memory_space=pl.ANY)
    dma = pltpu.SemaphoreType.DMA
    return pl.pallas_call(
        functools.partial(gather_kernel, n_sp, n_tp, group),
        out_shape=(
            jax.ShapeDtypeStruct((group * n_tp, rows, width), jnp.bfloat16),
            jax.ShapeDtypeStruct((n_sp,) + gates.shape, jnp.float32),
            jax.ShapeDtypeStruct((depth, out_rows, w_ret.shape[1]), jnp.bfloat16),
        ),
        in_specs=[vmem, vmem, vmem, hbm, hbm],
        out_specs=(hbm, vmem, hbm),
        scratch_shapes=[
            pltpu.VMEM((rows, width), jnp.bfloat16),
            dma((4,)),
            dma((max(group, 2),)),
            dma((max(group, 2),)),
            dma((3,)),
            dma((3,)),
            dma((group, n_tp)),
            dma((group, n_tp)),
            dma((n_sp,)),
            dma((n_sp,)),
            dma((depth,)),
            dma((depth,)),
            dma((depth,)),
            dma((depth,)),
        ],
        compiler_params=pltpu.CompilerParams(
            collective_id=0, has_side_effects=True, vmem_limit_bytes=VMEM_LIMIT
        ),
        name="gather",
    )(tokens, gain, gates, w_ret, w_fox)


def normalize(values):
    return (
        values * lax.rsqrt(jnp.mean(values * values, axis=1, keepdims=True) + eps)
    ).astype(jnp.bfloat16)


def mixer_kernel(
    n_sp,
    n_tp,
    group,
    rq,
    rk,
    rv,
    fq,
    fkv,
    gq,
    gk,
    within,
    qdec,
    kdec,
    bdec,
    wz,
    out,
    w_all,
    slots,
    raw,
    state,
    state_in,
    state_out,
    numer,
    denom,
    ret_buf,
    fox_buf,
    mixed,
    part,
    got,
    local_sem,
    ksend,
    krecv,
    ssend,
    srecv,
    wsend,
    wrecv,
    dsend,
    drecv,
    asend,
    arecv,
    osend,
    orecv,
):
    sp = lax.axis_index("sp")
    tp = lax.axis_index("tp")
    g = lax.rem(sp, group)
    z = sp // group
    depth = n_sp // group
    hret = rq.shape[0]
    hfox = fq.shape[0]
    run = rq.shape[1]
    tok = run // group
    rows = out.shape[0]
    after = lax.rem(sp + group, n_sp)
    before = lax.rem(sp + n_sp - group, n_sp)
    f32 = jnp.float32

    def peer(other):
        return z * group + other

    barrier = pltpu.get_barrier_semaphore()
    for i in range(1, group):
        pl.semaphore_signal(
            barrier, inc=1, device_id=(peer(lax.rem(g + i, group)), tp), device_id_type=MESH
        )
    for i in range(1, n_tp):
        pl.semaphore_signal(
            barrier, inc=1, device_id=(sp, lax.rem(tp + i, n_tp)), device_id_type=MESH
        )
    if depth > 1:

        @pl.when(z < depth - 1)
        def _():
            pl.semaphore_signal(barrier, inc=1, device_id=(after, tp), device_id_type=MESH)

        @pl.when(z > 0)
        def _():
            pl.semaphore_signal(barrier, inc=1, device_id=(before, tp), device_id_type=MESH)

    ends = (z + depth - 1) // depth + (2 * depth - 2 - z) // depth
    pl.semaphore_wait(barrier, group + n_tp - 2 + ends)

    def first_hop():
        return remote(fkv, slots.at[z], ksend.at[z], krecv.at[z], after, tp)

    def hop(block):
        return remote(
            slots.at[block], slots.at[block], ksend.at[block], krecv.at[block], after, tp
        )

    if depth > 1:

        @pl.when(z < depth - 1)
        def _():
            first_hop().start()

    hyper = group == 4
    mine = pltpu.make_async_copy(wz, w_all.at[g], local_sem.at[0])
    mine.start()
    direct = []
    for i in range(1, group):
        if hyper and i == 3:
            continue
        other = lax.bitwise_xor(g, i) if hyper else lax.rem(g + i, group)
        direct.append(
            remote(wz, w_all.at[g], wsend.at[i], wrecv.at[i], peer(other), tp)
        )
    for copy in direct:
        copy.start()

    def relay(i):
        source = lax.bitwise_xor(g, i)
        target = lax.bitwise_xor(g, 3 - i)
        span = pl.ds((i - 1) * (depth // 2), depth // 2)
        return remote(
            w_all.at[source, span],
            w_all.at[source, span],
            dsend.at[i],
            drecv.at[i],
            peer(target),
            tp,
        )

    for h in range(hret):
        state[h] = jnp.zeros(state.shape[1:], f32)

        def ret_step(b, carry):
            span = pl.ds(pl.multiple_of(b * BLOCK, BLOCK), BLOCK)
            q = rq[h, span, :]
            k = rk[h, span, :]
            v = rv[h, span, :]
            scores = (
                lax.dot_general(q, k, (((1,), (1,)), ((), ())), preferred_element_type=f32)
                * within[h]
            )
            inner = jnp.dot(scores.astype(jnp.bfloat16), v, preferred_element_type=f32)
            held = state[h]
            cross = jnp.dot(q, held.astype(jnp.bfloat16), preferred_element_type=f32)
            raw[h, span, :] = inner + cross * qdec[h, pl.ds(0, BLOCK), :]
            scaled = (k.astype(f32) * kdec[h]).astype(jnp.bfloat16)
            update = lax.dot_general(
                scaled, v, (((0,), (0,)), ((), ())), preferred_element_type=f32
            )
            state[h] = held * bdec[h, 0:1, :] + update
            return carry

        lax.fori_loop(0, run // BLOCK, ret_step, 0)

    def state_hop():
        return remote(state_out, state_in, ssend.at[0], srecv.at[0], after, tp)

    if depth > 1:

        @pl.when(z == 0)
        def _():
            state_out[...] = state[...]
            state_hop().start()

    tile = math.gcd(run, 256)
    inverse = FOX_DIM ** (-0.5)

    def attend(h, t, keys, values, key_gates, diagonal, fresh):
        span = pl.ds(pl.multiple_of(t * tile, tile), tile)
        scores = (
            lax.dot_general(
                fq[h, span, :], keys, (((1,), (1,)), ((), ())), preferred_element_type=f32
            )
            * inverse
        )
        scores = scores + gq[h, span, :] - key_gates
        if diagonal:
            row = lax.broadcasted_iota(jnp.int32, scores.shape, 0)
            col = lax.broadcasted_iota(jnp.int32, scores.shape, 1)
            scores = jnp.where(col <= row, scores, -jnp.inf)
        weights = jnp.exp(scores)
        total = jnp.sum(weights, axis=1, keepdims=True)
        product = jnp.dot(weights.astype(jnp.bfloat16), values, preferred_element_type=f32)
        if fresh:
            numer[h, span, :] = product
            denom[h, span, :] = total
        else:
            numer[h, span, :] += product
            denom[h, span, :] += total

    for h in range(hfox):
        for t in range(run // tile):
            for s in range(t, -1, -1):
                span = pl.ds(s * tile, tile)
                attend(
                    h,
                    t,
                    fkv[0, h, span, :],
                    fkv[1, h, span, :],
                    gk[h, z, :, span],
                    s == t,
                    s == t,
                )

    def carried():
        state_hop().wait_recv()

        @pl.when(z < depth - 1)
        def _():
            for h in range(hret):
                state_out[h] = state_in[h] * bdec[h, 1:2, :] + state[h]
            state_hop().start()

        for h in range(hret):
            held = state_in[h].astype(jnp.bfloat16)

            def cross_step(b, carry):
                span = pl.ds(pl.multiple_of(b * tile, tile), tile)
                cross = jnp.dot(rq[h, span, :], held, preferred_element_type=f32)
                raw[h, span, :] += cross * qdec[h, span, :]
                return carry

            lax.fori_loop(0, run // tile, cross_step, 0)

    def earlier(step, carry):
        @pl.when(step <= z)
        def _():
            block = z - step
            hop(block).wait_recv()

            @pl.when(z < depth - 1)
            def _():
                hop(block).start()

            for h in range(hfox):

                def query_step(t, c):
                    attend(
                        h,
                        t,
                        slots[block, 0, h],
                        slots[block, 1, h],
                        gk[h, block],
                        False,
                        False,
                    )
                    return c

                lax.fori_loop(0, run // tile, query_step, 0)

        return carry

    if depth > 1:
        lax.fori_loop(1, 2, earlier, 0)

        @pl.when(z > 0)
        def _():
            carried()

        if hyper:
            direct[0].wait_recv()
            relay(1).start()
            direct[1].wait_recv()
            relay(2).start()
        lax.fori_loop(2, depth, earlier, 0)
    elif hyper:
        direct[0].wait_recv()
        relay(1).start()
        direct[1].wait_recv()
        relay(2).start()

    rw = hret * RET_DIM
    fw = hfox * FOX_DIM
    for t in range(group):
        span = pl.ds(t * tok, tok)
        for h in range(hret):
            ret_buf[t, :, h * RET_DIM : (h + 1) * RET_DIM] = normalize(raw[h, span, :])
        for h in range(hfox):
            fox_buf[t, :, h * FOX_DIM : (h + 1) * FOX_DIM] = normalize(
                numer[h, span, :] / denom[h, span, :]
            )
    ret_cols = pl.ds(pl.multiple_of(g * rw, 128), rw)
    fox_cols = pl.ds(pl.multiple_of(group * rw + g * fw, 128), fw)
    exchange = []
    for i in range(1, group):
        other = lax.rem(g + i, group)
        for kind, (buf, cols) in enumerate(((ret_buf, ret_cols), (fox_buf, fox_cols))):
            copy = remote(
                buf.at[other],
                mixed.at[:, cols],
                asend.at[kind, i],
                arecv.at[kind, i],
                peer(other),
                tp,
            )
            copy.start()
            exchange.append(copy)
    mixed[:, ret_cols] = ret_buf[g]
    mixed[:, fox_cols] = fox_buf[g]
    for copy in exchange:
        copy.wait_recv()
    mine.wait()
    if hyper:
        relay(1).wait_recv()
        relay(2).wait_recv()
    else:
        for copy in direct:
            copy.wait_recv()

    cols = w_all.shape[3]
    pack = max(1, 128 // cols)
    wide = pack * cols
    for t in range(n_tp):
        left = mixed[t * rows : (t + 1) * rows, :]

        def column(p, carry, left=left, t=t):
            blocks = [
                w_all[lax.rem(p * pack + i, group), (p * pack + i) // group]
                for i in range(pack)
            ]
            right = blocks[0] if pack == 1 else jnp.concatenate(blocks, axis=1)
            product = jnp.dot(left, right, preferred_element_type=f32)
            at = pl.ds(pl.multiple_of(p * wide, wide), wide)
            part[t, :, at] = product.astype(jnp.bfloat16)
            return carry

        lax.fori_loop(0, n_sp // pack, column, 0)
    final = []
    for i in range(1, n_tp):
        other = lax.rem(tp + i, n_tp)
        copy = remote(part.at[other], got.at[i], osend.at[i], orecv.at[i], sp, other)
        copy.start()
        final.append(copy)
    total = part[tp].astype(f32)
    for i in range(1, n_tp):
        final[i - 1].wait_recv()
        total = total + got[i].astype(f32)
    out[...] = total.astype(jnp.bfloat16)

    for copy in final + exchange + direct:
        copy.wait_send()
    if hyper:
        relay(1).wait_send()
        relay(2).wait_send()
    if depth > 1:

        @pl.when(z < depth - 1)
        def _():
            first_hop().wait_send()
            state_hop().wait_send()

            def settle(block, carry):
                @pl.when(block < z)
                def _():
                    hop(block).wait_send()

                return carry

            lax.fori_loop(0, depth, settle, 0)


def mixer(rq, rk, rv, fq, fkv, gq, gk, within, qdec, kdec, bdec, wz, rows, n_sp, n_tp, group):
    depth = n_sp // group
    hret, run, _ = rq.shape
    hfox = fq.shape[0]
    tok = run // group
    out_rows, cols = wz.shape[1:]
    width = n_sp * cols
    vmem = pl.BlockSpec(memory_space=pltpu.VMEM)
    dma = pltpu.SemaphoreType.DMA
    f32 = jnp.float32
    bf16 = jnp.bfloat16
    square = (hret, RET_DIM, RET_DIM)
    return pl.pallas_call(
        functools.partial(mixer_kernel, n_sp, n_tp, group),
        out_shape=jax.ShapeDtypeStruct((rows, width), bf16),
        in_specs=[vmem] * 11 + [pl.BlockSpec(memory_space=pl.ANY)],
        out_specs=vmem,
        scratch_shapes=[
            pltpu.VMEM((group,) + wz.shape, bf16),
            pltpu.VMEM((depth,) + fkv.shape, bf16),
            pltpu.VMEM((hret, run, RET_DIM), f32),
            pltpu.VMEM(square, f32),
            pltpu.VMEM(square, f32),
            pltpu.VMEM(square, f32),
            pltpu.VMEM((hfox, run, FOX_DIM), f32),
            pltpu.VMEM((hfox, run, 1), f32),
            pltpu.VMEM((group, tok, hret * RET_DIM), bf16),
            pltpu.VMEM((group, tok, hfox * FOX_DIM), bf16),
            pltpu.VMEM((tok, out_rows), bf16),
            pltpu.VMEM((n_tp, rows, width), bf16),
            pltpu.VMEM((n_tp, rows, width), bf16),
            dma((1,)),
            dma((depth,)),
            dma((depth,)),
            dma((1,)),
            dma((1,)),
            dma((max(group, 2),)),
            dma((max(group, 2),)),
            dma((3,)),
            dma((3,)),
            dma((2, group)),
            dma((2, group)),
            dma((n_tp,)),
            dma((n_tp,)),
        ],
        compiler_params=pltpu.CompilerParams(
            collective_id=1, has_side_effects=True, vmem_limit_bytes=VMEM_LIMIT
        ),
        name="mixer",
    )(rq, rk, rv, fq, fkv, gq, gk, within, qdec, kdec, bdec, wz)


def decay_rates(head_ids, total):
    heads_float = head_ids.astype(jnp.float32)
    middle = RET_HEADS // 2
    fast_rate = 1.0 / (32.0 + 16.0 * heads_float)
    slow_rate = jnp.exp2(-(heads_float - middle)) / total
    return jnp.where(head_ids < middle, fast_rate, slow_rate)


def per_device(
    n_sp,
    n_tp,
    tokens,
    gain,
    w_ret_q,
    w_ret_k,
    w_ret_v,
    w_fox_q,
    w_fox_k,
    w_fox_v,
    fox_gates,
    w_out_ret,
    w_out_fox,
):
    f32 = jnp.float32
    bf16 = jnp.bfloat16
    rows, width = tokens.shape
    ret_heads = w_ret_q.shape[1] // RET_DIM
    fox_heads = w_fox_q.shape[1] // FOX_DIM
    group = math.gcd(math.gcd(ret_heads, fox_heads), n_sp)
    depth = n_sp // group
    hret = ret_heads // group
    hfox = fox_heads // group
    run = rows * n_tp * group
    sp = lax.axis_index("sp")
    g = lax.rem(sp, group)
    z = sp // group

    xall, gall, wz = gather(
        tokens, gain.reshape(1, width), fox_gates.T, w_out_ret, w_out_fox, n_sp, n_tp, group
    )
    x = xall.reshape(run, width)

    def project(matrix, heads, size):
        cut = lax.dynamic_slice_in_dim(matrix, g * heads * size, heads * size, 1)
        return jnp.dot(x, cut, preferred_element_type=f32).astype(bf16)

    def split(values, size):
        return values.reshape(run, -1, size).transpose(1, 0, 2)

    positions = z * run + jnp.arange(run, dtype=jnp.int32)
    half = RET_DIM // 2
    inverse = 10000.0 ** (-jnp.arange(half, dtype=f32) / half)
    angles = positions.astype(f32)[:, None] * inverse[None, :]
    cosine = jnp.cos(angles)[None]
    sine = jnp.sin(angles)[None]

    def rotate(values):
        wide = values.astype(f32)
        a = wide[..., :half]
        b = wide[..., half:]
        return jnp.concatenate([a * cosine - b * sine, a * sine + b * cosine], axis=-1)

    rq = rotate(split(project(w_ret_q, hret, RET_DIM), RET_DIM)).astype(bf16)
    rk = (
        rotate(split(project(w_ret_k, hret, RET_DIM), RET_DIM)) * RET_DIM ** (-0.5)
    ).astype(bf16)
    rv = split(project(w_ret_v, hret, RET_DIM), RET_DIM)
    fq = split(project(w_fox_q, hfox, FOX_DIM), FOX_DIM)
    fk = split(project(w_fox_k, hfox, FOX_DIM), FOX_DIM)
    fv = split(project(w_fox_v, hfox, FOX_DIM), FOX_DIM)
    fkv = jnp.stack([fk, fv])

    head_ids = (
        lax.axis_index("tp") * ret_heads + g * hret + jnp.arange(hret, dtype=jnp.int32)
    )
    rates = decay_rates(head_ids, float(run * depth))
    offsets = jnp.arange(BLOCK, dtype=f32)
    spread = offsets[:, None] - offsets[None, :]
    causal = spread >= 0
    within = jnp.where(
        causal[None], jnp.exp(-rates[:, None, None] * jnp.where(causal, spread, 0.0)[None]), 0.0
    )
    steps = jnp.arange(run, dtype=f32)
    qdec = jnp.exp(-rates[:, None] * (steps[None, :] + 1.0))[:, :, None]
    kdec = jnp.exp(-rates[:, None] * (BLOCK - 1.0 - offsets[None, :]))[:, :, None]
    lengths = jnp.array([BLOCK, run], f32)
    bdec = jnp.broadcast_to(
        jnp.exp(-rates[:, None] * lengths[None, :])[:, :, None], (hret, 2, RET_DIM)
    )

    own_gates = lax.dynamic_slice_in_dim(gall, g * hfox, hfox, 1)
    line = own_gates.transpose(1, 0, 2).reshape(hfox, depth, 1, run)
    gq = lax.dynamic_index_in_dim(line, z, 1, False).reshape(hfox, run, 1)
    return mixer(
        rq, rk, rv, fq, fkv, gq, line, within, qdec, kdec, bdec, wz, rows, n_sp, n_tp, group
    )


def solution(mesh):
    in_specs = (
        P(("sp", "tp"), None),
        P(),
        P(None, "tp"),
        P(None, "tp"),
        P(None, "tp"),
        P(None, "tp"),
        P(None, "tp"),
        P(None, "tp"),
        P("sp", "tp"),
        P("tp", "sp"),
        P("tp", "sp"),
    )
    out_specs = P(("sp", "tp"), None)
    return jax.shard_map(
        functools.partial(per_device, mesh.shape["sp"], mesh.shape["tp"]),
        mesh=mesh,
        in_specs=in_specs,
        out_specs=out_specs,
        check_vma=False,
    )
```

time: 544 us -> 158 us (0.29)
  waiting for transfers between devices: 376 us -> 0 us
  Pallas kernels: 0 us -> 126 us
  blocking collectives: 77.7 us -> 0 us
  local copies, waits for them, and re-layouts: 27.5 us -> 4.47 us
  matrix products: 36.2 us -> 19.6 us
  between operations: 13.8 us -> 0.24 us
  loops' own time: 5.99 us -> 0 us
    all_gather x6 -> x0, waiting for transfers between devices: 368 us -> none  [the longest x1 172 us: prefix(): gathered = jax.tree.map(lambda a: lax.all_gather(a, axis), part)]
    pallas_call x0 -> x2, Pallas kernels: none -> 126 us  [the longest x1 77 us: mixer(): pl.pallas_call(functools.partial(mixer_kernel, n_sp, n_tp, group), out_sh...]
    all_gather x2 -> x0, blocking collectives: 77.7 us -> none  [the longest x1 41.5 us: prefix(): gathered = jax.tree.map(lambda a: lax.all_gather(a, axis), part)]
    dot_general x18 -> x6, matrix products: 36.2 us -> 19.6 us  [project(): return jnp.dot(x, cut, preferred_element_type=f32).astype(bf16)]
    unnamed x17 -> x11, local copies, waits for them, and re-layouts: 14.3 us -> 1.9 us
    reduce_scatter x1 -> x0, waiting for transfers between devices: 6.73 us -> none  [per_device(): lax.psum_scatter((jnp.dot(ret_mixed, out_ret, preferred_element_type=jnp....]
    dynamic_slice x13 -> x1, local copies, waits for them, and re-layouts: 6.95 us -> 0.85 us  [per_device(): own_gates = lax.dynamic_slice_in_dim(gall, g * hfox, hfox, 1)]
    another operation x12 -> x0, loops' own time: 5.99 us -> none  [the longest x1 5.52 us: per_device(): lax.scan(one_block, (zero_numer, zero_denom), jnp.arange(rows_here // wid...]
  transfers between devices with their start and end apart: 7 -> 0, of which waited for: 6 -> 0; matrix products, arithmetic and copies ran while one was open for 11% -> 0% of each run, Pallas kernels for 0% -> 0%
where the time goes in v1:
time: 158 us; the launch traced here: 157 us
  Pallas kernels  126 us (80%)
  matrix products  19.6 us (12%)
  other arithmetic  7.35 us (5%)
  local copies, waits for them, and re-layouts  4.47 us (3%)
    pallas_call x1, Pallas kernels, mixer(): pl.pallas_call(functools.partial(mixer_kernel, n_sp, n_tp, group), out_sh...  77 us
    pallas_call x1, Pallas kernels, gather(): pl.pallas_call(functools.partial(gather_kernel, n_sp, n_tp, group), out_s...  48.6 us
    dot_general x6, matrix products, project(): return jnp.dot(x, cut, preferred_element_type=f32).astype(bf16)  19.6 us

profile of v1, /device:TPU:0, one launch (start us, length us, event | category | flops | bytes accessed | tf_op | source)
XLA Modules:
  0.0 157.4 jit_solution(3601525072866210399)
XLA Ops:
  0.0 0.0 copy-start
  0.0 48.6 %gather.1 = (bf16[8,128,2048]{2,1,0:T(8,128)(2,1)}, f32[16,4,256]{2,1,0:T(4,128)}, bf16[4,1536,128]{2,1,0:T(8,128)(2,1)}) custom-call(bf16[128,2048]{1,0:T(8,128)(2,1)} %tok_ref.1, f32[1,2048]{1,0:T(1,128)} %bitcast.32, f32[4,256]{1,0:T(4,128)} %bitcast.33, bf16[1024,128]{1,0:T(8,128)(2,1)} %wr_ref.1, bf16[512,128]{1,0:T(8,128)(2,1)} %wf_ref.1), custom_call_target="tpu_custom_call" | custom-call | tf_op jit(solution)/shard_map/gather/pallas_call | solution.py:254
  48.7 3.7 %fusion.3 = f32[1,1024,256]{2,1,0:T(8,128)S(1)} fusion(bf16[1024,2048]{1,0:T(8,128)(2,1)} %bitcast.34, bf16[2048,1024]{1,0:T(8,128)(2,1)} %param.15, s32[]{:T(128)S(6)} %select_n.41), kind=kOutput, calls=%fused_computation.6 | convolution fusion | flops 1074266112 | bytes 6291460 | tf_op jit(solution)/shard_map/dot_general | solution.py:744
  52.4 3.7 %fusion.1 = f32[1,1024,256]{2,1,0:T(8,128)S(1)} fusion(bf16[1024,2048]{1,0:T(8,128)(2,1)} %bitcast.35, bf16[2048,1024]{1,0:T(8,128)(2,1)} %param.14, s32[]{:T(128)S(6)} %select_n.41), kind=kOutput, calls=%fused_computation.4 | convolution fusion | flops 1074266112 | bytes 6291460 | tf_op jit(solution)/shard_map/dot_general | solution.py:744
  56.2 0.0 copy-start.2
  56.2 2.5 %fusion.24 = (f32[1,1024,128]{2,1,0:T(8,128)S(1)}, f32[1,1024,128]{2,1,0:T(8,128)S(1)}, bf16[1,1024,128]{2,1,0:T(8,128)(2,1)S(1)}, bf16[1,1024,128]{2,1,0:T(8,128)(2,1)S(1)}) fusion(f32[1,1024,256]{2,1,0:T(8,128)S(1)} %fusion.3, f32[128]{0:T(128)S(1)} %multiply_power_fusion, f32[1024]{0:T(1024)S(1)} %add_convert_fusion, f32[1,1024,256]{2,1,0:T(8,128)S(1)} %fusion.1), kind=kLoop, calls=%fused_computation.33 | loop fusion | flops 1966080 | bytes 3674624 | tf_op jit(solution)/shard_map/sub | solution.py:760
  58.7 0.9 pad_maximum_fusion.rq
  59.5 0.9 fusion.8.rk
  60.4 3.3 %fusion.4.rv = bf16[1,1024,256]{2,1,0:T(8,128)(2,1)} fusion(bf16[1024,2048]{1,0:T(8,128)(2,1)S(1)} %bitcast.37, bf16[2048,1024]{1,0:T(8,128)(2,1)} %param.16, s32[]{:T(128)S(6)} %select_n.41), kind=kOutput, calls=%fused_computation.7 | convolution fusion | flops 1074003968 | bytes 5767172 | tf_op jit(solution)/shard_map/dot_general | solution.py:744
  63.7 4.3 %fusion.5.fq = bf16[1,1024,128]{2,1,0:T(8,128)(2,1)} fusion(bf16[1024,2048]{1,0:T(8,128)(2,1)} %bitcast.36, bf16[2048,512]{1,0:T(8,128)(2,1)S(1)} %copy-done, s32[]{:T(128)S(6)} %select_n.43), kind=kOutput, calls=%fused_computation.11 | convolution fusion | flops 537001984 | bytes 4980740 | tf_op jit(solution)/shard_map/dot_general | solution.py:744
  68.0 2.3 %fusion.7 = bf16[1,1,1024,128]{3,2,1,0:T(8,128)(2,1)S(1)} fusion(bf16[1024,2048]{1,0:T(8,128)(2,1)S(1)} %bitcast.38, bf16[2048,512]{1,0:T(8,128)(2,1)} %param.19, s32[]{:T(128)S(6)} %select_n.43), kind=kOutput, calls=%fused_computation.13 | convolution fusion | flops 537001984 | bytes 4980740 | tf_op jit(solution)/shard_map/dot_general | solution.py:744
  70.3 0.0 copy-start.4
  70.3 2.3 %fusion.6 = bf16[1,1,1024,128]{3,2,1,0:T(8,128)(2,1)S(1)} fusion(bf16[1024,2048]{1,0:T(8,128)(2,1)S(1)} %bitcast.39, bf16[2048,512]{1,0:T(8,128)(2,1)} %param.18, s32[]{:T(128)S(6)} %select_n.43), kind=kOutput, calls=%fused_computation.12 | convolution fusion | flops 537001984 | bytes 4980740 | tf_op jit(solution)/shard_map/dot_general | solution.py:744
  72.6 0.8 pad_maximum_fusion.1.fkv
  73.4 0.9 constant_dynamic-slice_fusion
  74.3 0.0 copy-start.1
  74.3 1.0 copy.22.gq
  75.4 0.7 compare_select_fusion.within
  76.1 1.0 multiply_exponential_fusion.qdec
  77.1 0.7 multiply_exponential_fusion.1.kdec
  77.8 0.0 copy-done.4
  77.8 0.7 broadcast_in_dim.4.bdec
  78.4 77.0 %mixer.1 = bf16[128,2048]{1,0:T(8,128)(2,1)} custom-call(bf16[1,1024,256]{2,1,0:T(8,128)(2,1)} %pad_maximum_fusion.rq, bf16[1,1024,256]{2,1,0:T(8,128)(2,1)} %fusion.8.rk, bf16[1,1024,256]{2,1,0:T(8,128)(2,1)} %fusion.4.rv, bf16[1,1024,128]{2,1,0:T(8,128)(2,1)} %fusion.5.fq, bf16[2,1,1024,128]{3,2,1,0:T(8,128)(2,1)} %pad_maximum_fusion.1.fkv, ...), custom_call_target="tpu_custom_call" | custom-call | tf_op jit(solution)/shard_map/mixer/pallas_call | solution.py:660
  155.5 1.9 %copy.26 = bf16[128,2048]{1,0:T(8,128)(2,1)} copy(bf16[128,2048]{1,0:T(8,128)(2,1)} %mixer.1) | data formatting | bytes 1048576
  (9 shorter events, 0.0 us)
Async XLA Ops:
  0.0 63.7 %copy-start = (bf16[2048,512]{1,0:T(8,128)(2,1)S(1)}, bf16[2048,512]{1,0:T(8,128)(2,1)}, u32[]{:S(2)}) copy-start(bf16[2048,512]{1,0:T(8,128)(2,1)} %param.17) | copy-start | bytes 6291460
  56.2 4.2 %copy-start.2 = (bf16[8,128,2048]{2,1,0:T(8,128)(2,1)S(1)}, bf16[8,128,2048]{2,1,0:T(8,128)(2,1)}, u32[]{:S(2)}) copy-start(bf16[8,128,2048]{2,1,0:T(8,128)(2,1)} %get-tuple-element.8) | copy-start | bytes 12582916
  63.7 4.3 %copy-start.3 = (bf16[8,128,2048]{2,1,0:T(8,128)(2,1)S(1)}, bf16[8,128,2048]{2,1,0:T(8,128)(2,1)}, u32[]{:S(2)}) copy-start(bf16[8,128,2048]{2,1,0:T(8,128)(2,1)} %get-tuple-element.8) | copy-start | bytes 12582916
  70.3 7.5 %copy-start.4 = (f32[2]{0:T(128)S(1)}, f32[2]{0:T(128)}, u32[]{:S(2)}) copy-start(f32[2]{0:T(128)} %constant.74.clone) | copy-start | bytes 28
  74.3 4.2 %copy-start.1 = (f32[16,1,256]{2,1,0:T(1,128)}, f32[16,1,256]{2,1,0:T(1,128)S(1)}, u32[]{:S(2)}) copy-start(f32[16,1,256]{2,1,0:T(1,128)S(1)} %constant_dynamic-slice_fusion) | copy-start | bytes 49156

commit v2 on v1

--- a/solution.py
+++ b/solution.py
@@ -38,11 +38,22 @@
     gates_ref,
     wr_ref,
     wf_ref,
-    xall,
+    cos_ref,
+    sin_ref,
+    w_in,
+    rq,
+    rk,
+    rv,
+    fq,
+    fkv,
     gall,
     wz,
     own,
+    xall,
+    w_ret,
+    w_fox,
     local_sem,
+    in_sem,
     tsend,
     trecv,
     dsend,
@@ -75,6 +86,15 @@
             barrier, inc=1, device_id=(sp, lax.rem(tp + i, n_tp)), device_id_type=MESH
         )
 
+    loads = []
+    for i in range(6):
+        cut = w_ret if i < 3 else w_fox
+        size = cut.shape[2]
+        columns = pl.ds(pl.multiple_of(g * size, 128), size)
+        loads.append(
+            pltpu.make_async_copy(w_in[i].at[:, columns], cut.at[i % 3], in_sem.at[i])
+        )
+
     values = tok_ref[...].astype(jnp.float32)
     scale = lax.rsqrt(jnp.mean(values * values, axis=1, keepdims=True) + eps)
     own[...] = (values * scale * gain_ref[...]).astype(jnp.bfloat16)
@@ -85,7 +105,7 @@
         ),
         pltpu.make_async_copy(gates_ref, gall.at[sp], local_sem.at[2]),
     ]
-    for copy in copies:
+    for copy in copies + loads:
         copy.start()
     pl.semaphore_wait(barrier, n_sp + n_tp - 2)
 
@@ -155,7 +175,10 @@
     def _():
         down(z).start()
 
+    ready = {0: pair[:]}
+
     def forward(which, row):
+        ready[row] = []
         for i in range(1, n_tp):
             copy = remote(
                 slot(which, tp),
@@ -167,6 +190,46 @@
             )
             copy.start()
             pair.append(copy)
+            ready[row].append(copy)
+
+    count = n_tp * rows
+    half_head = RET_DIM // 2
+
+    def project(which, row):
+        for copy in ready[row]:
+            copy.wait_recv()
+        x = xall[pl.ds(which * n_tp, n_tp)].reshape(count, xall.shape[2])
+        span = pl.ds(pl.multiple_of(which * count, count), count)
+        for i in range(6):
+            cut = w_ret if i < 3 else w_fox
+            y = jnp.dot(x, cut[i % 3], preferred_element_type=jnp.float32)
+            y = y.astype(jnp.bfloat16)
+            if i < 2:
+                cosine = cos_ref[span, :]
+                sine = sin_ref[span, :]
+            for h in range(rq.shape[0] if i < 3 else fq.shape[0]):
+                if i < 2:
+                    lo = h * RET_DIM
+                    a = y[:, lo : lo + half_head].astype(jnp.float32)
+                    b = y[:, lo + half_head : lo + RET_DIM].astype(jnp.float32)
+                    to = rq if i == 0 else rk
+                    by = 1.0 if i == 0 else RET_DIM ** (-0.5)
+                    first = (a * cosine - b * sine) * by
+                    second = (a * sine + b * cosine) * by
+                    to[h, span, :half_head] = first.astype(jnp.bfloat16)
+                    to[h, span, half_head:] = second.astype(jnp.bfloat16)
+                elif i == 2:
+                    rv[h, span, :] = y[:, h * RET_DIM : (h + 1) * RET_DIM]
+                elif i == 3:
+                    fq[h, span, :] = y[:, h * FOX_DIM : (h + 1) * FOX_DIM]
+                else:
+                    fkv[i - 4, h, span, :] = y[:, h * FOX_DIM : (h + 1) * FOX_DIM]
+
+    mine.wait()
+    for copy in loads:
+        copy.wait()
+    if not hyper:
+        project(g, 0)
 
     if hyper:
         relays = []
@@ -186,10 +249,12 @@
             copy.start()
             relays.append(copy)
             forward(source, i)
+        project(g, 0)
     else:
         for i in range(1, group):
             direct[i - 1].wait_recv()
             forward(lax.rem(g + group - i, group), i)
+            project(lax.rem(g + group - i, group), i)
 
     def line(step, carry):
         below = z - step
@@ -216,10 +281,15 @@
     split = depth // 2 if hyper else depth
     lax.fori_loop(1, split, line, 0)
     if hyper:
+        project(lax.bitwise_xor(g, 1), 1)
         for copy in relays:
             copy.wait_recv()
         forward(lax.bitwise_xor(g, 3), 3)
-    lax.fori_loop(split, depth, line, 0)
+    lax.fori_loop(split, depth - 1, line, 0)
+    if hyper:
+        project(lax.bitwise_xor(g, 2), 2)
+        project(lax.bitwise_xor(g, 3), 3)
+    lax.fori_loop(max(split, depth - 1), depth, line, 0)
 
     def settle(step, carry):
         @pl.when((z < depth - 1) & (step <= z))
@@ -238,31 +308,48 @@
     if hyper:
         for copy in relays:
             copy.wait_send()
-    for copy in gate_copies + pair:
+    for copy in gate_copies:
         copy.wait()
+    for copy in pair:
+        copy.wait_send()
     copies[2].wait()
-    mine.wait()
-
-
-def gather(tokens, gain, gates, w_ret, w_fox, n_sp, n_tp, group):
+
+
+def gather(
+    tokens, gain, gates, w_ret, w_fox, cosine, sine, w_in, hret, hfox, n_sp, n_tp, group
+):
     rows, width = tokens.shape
     depth = n_sp // group
     out_rows = w_ret.shape[0] + w_fox.shape[0]
     vmem = pl.BlockSpec(memory_space=pltpu.VMEM)
     hbm = pl.BlockSpec(memory_space=pl.ANY)
     dma = pltpu.SemaphoreType.DMA
+    run = rows * n_tp * group
+    bf16 = jnp.bfloat16
+
+    def body(*refs):
+        gather_kernel(n_sp, n_tp, group, *refs[:7], refs[7:13], *refs[13:])
+
     return pl.pallas_call(
-        functools.partial(gather_kernel, n_sp, n_tp, group),
+        body,
         out_shape=(
-            jax.ShapeDtypeStruct((group * n_tp, rows, width), jnp.bfloat16),
+            jax.ShapeDtypeStruct((hret, run, RET_DIM), bf16),
+            jax.ShapeDtypeStruct((hret, run, RET_DIM), bf16),
+            jax.ShapeDtypeStruct((hret, run, RET_DIM), bf16),
+            jax.ShapeDtypeStruct((hfox, run, FOX_DIM), bf16),
+            jax.ShapeDtypeStruct((2, hfox, run, FOX_DIM), bf16),
             jax.ShapeDtypeStruct((n_sp,) + gates.shape, jnp.float32),
             jax.ShapeDtypeStruct((depth, out_rows, w_ret.shape[1]), jnp.bfloat16),
         ),
-        in_specs=[vmem, vmem, vmem, hbm, hbm],
-        out_specs=(hbm, vmem, hbm),
+        in_specs=[vmem, vmem, vmem, hbm, hbm, vmem, vmem] + [hbm] * 6,
+        out_specs=(vmem,) * 7,
         scratch_shapes=[
-            pltpu.VMEM((rows, width), jnp.bfloat16),
+            pltpu.VMEM((rows, width), bf16),
+            pltpu.VMEM((group * n_tp, rows, width), bf16),
+            pltpu.VMEM((3, width, hret * RET_DIM), bf16),
+            pltpu.VMEM((3, width, hfox * FOX_DIM), bf16),
             dma((4,)),
+            dma((6,)),
             dma((max(group, 2),)),
             dma((max(group, 2),)),
             dma((3,)),
@@ -280,7 +367,7 @@
             collective_id=0, has_side_effects=True, vmem_limit_bytes=VMEM_LIMIT
         ),
         name="gather",
-    )(tokens, gain, gates, w_ret, w_fox)
+    )(tokens, gain, gates, w_ret, w_fox, cosine, sine, *w_in)
 
 
 def normalize(values):
@@ -721,7 +808,6 @@
     w_out_fox,
 ):
     f32 = jnp.float32
-    bf16 = jnp.bfloat16
     rows, width = tokens.shape
     ret_heads = w_ret_q.shape[1] // RET_DIM
     fox_heads = w_fox_q.shape[1] // FOX_DIM
@@ -734,40 +820,25 @@
     g = lax.rem(sp, group)
     z = sp // group
 
-    xall, gall, wz = gather(
-        tokens, gain.reshape(1, width), fox_gates.T, w_out_ret, w_out_fox, n_sp, n_tp, group
-    )
-    x = xall.reshape(run, width)
-
-    def project(matrix, heads, size):
-        cut = lax.dynamic_slice_in_dim(matrix, g * heads * size, heads * size, 1)
-        return jnp.dot(x, cut, preferred_element_type=f32).astype(bf16)
-
-    def split(values, size):
-        return values.reshape(run, -1, size).transpose(1, 0, 2)
-
     positions = z * run + jnp.arange(run, dtype=jnp.int32)
     half = RET_DIM // 2
     inverse = 10000.0 ** (-jnp.arange(half, dtype=f32) / half)
     angles = positions.astype(f32)[:, None] * inverse[None, :]
-    cosine = jnp.cos(angles)[None]
-    sine = jnp.sin(angles)[None]
-
-    def rotate(values):
-        wide = values.astype(f32)
-        a = wide[..., :half]
-        b = wide[..., half:]
-        return jnp.concatenate([a * cosine - b * sine, a * sine + b * cosine], axis=-1)
-
-    rq = rotate(split(project(w_ret_q, hret, RET_DIM), RET_DIM)).astype(bf16)
-    rk = (
-        rotate(split(project(w_ret_k, hret, RET_DIM), RET_DIM)) * RET_DIM ** (-0.5)
-    ).astype(bf16)
-    rv = split(project(w_ret_v, hret, RET_DIM), RET_DIM)
-    fq = split(project(w_fox_q, hfox, FOX_DIM), FOX_DIM)
-    fk = split(project(w_fox_k, hfox, FOX_DIM), FOX_DIM)
-    fv = split(project(w_fox_v, hfox, FOX_DIM), FOX_DIM)
-    fkv = jnp.stack([fk, fv])
+    rq, rk, rv, fq, fkv, gall, wz = gather(
+        tokens,
+        gain.reshape(1, width),
+        fox_gates.T,
+        w_out_ret,
+        w_out_fox,
+        jnp.cos(angles),
+        jnp.sin(angles),
+        (w_ret_q, w_ret_k, w_ret_v, w_fox_q, w_fox_k, w_fox_v),
+        hret,
+        hfox,
+        n_sp,
+        n_tp,
+        group,
+    )
 
     head_ids = (
         lax.axis_index("tp") * ret_heads + g * hret + jnp.arange(hret, dtype=jnp.int32)

time: 158 us -> 129 us (0.82)
  matrix products: 19.6 us -> 0 us
  Pallas kernels: 126 us -> 118 us
  other arithmetic: 7.35 us -> 5.37 us
    dot_general x6 -> x0, matrix products: 19.6 us -> none  [project(): return jnp.dot(x, cut, preferred_element_type=f32).astype(bf16)]
    pallas_call x1, Pallas kernels: 48.6 us -> 43.2 us  [gather(): pl.pallas_call(body, out_shape=(jax.ShapeDtypeStruct((hret, run, RET_DIM)...]
    sin x0 -> x1, other arithmetic: none -> 3.05 us  [per_device(): jnp.sin(angles)]
    sub x1 -> x0, other arithmetic: 2.46 us -> none  [rotate(): a * cosine - b * sine]
    pallas_call x1, Pallas kernels: 77 us -> 75.2 us  [mixer(): pl.pallas_call(functools.partial(mixer_kernel, n_sp, n_tp, group), out_sh...]
where the time goes in v2:
time: 129 us; the launch traced here: 128 us
  Pallas kernels  118 us (91%)
  other arithmetic  5.37 us (4%)
  local copies, waits for them, and re-layouts  4.44 us (3%)
    pallas_call x1, Pallas kernels, mixer(): pl.pallas_call(functools.partial(mixer_kernel, n_sp, n_tp, group), out_sh...  75.2 us
    pallas_call x1, Pallas kernels, gather(): pl.pallas_call(body, out_shape=(jax.ShapeDtypeStruct((hret, run, RET_DIM)...  43.2 us
    sin x1, other arithmetic, per_device(): jnp.sin(angles)  3.05 us

profile of v2, /device:TPU:0, one launch (start us, length us, event | category | flops | bytes accessed | tf_op | source)
XLA Modules:
  0.0 128.4 jit_solution(10052814378817212886)
XLA Ops:
  0.0 3.1 %multiply_sine_fusion = (f32[1024,128]{1,0:T(8,128)}, f32[1024,128]{1,0:T(8,128)}) fusion(f32[128]{0:T(128)S(1)} %multiply_power_fusion, f32[1024]{0:T(1024)S(1)} %add_convert_fusion), kind=kLoop, calls=%fused_computation | loop fusion | flops 131072 | bytes 1053184 | tf_op jit(solution)/shard_map/sin | solution.py:834
  3.1 0.0 copy-start.1
  3.1 43.2 %gather.1 = (bf16[1,1024,256]{2,1,0:T(8,128)(2,1)}, bf16[1,1024,256]{2,1,0:T(8,128)(2,1)}, bf16[1,1024,256]{2,1,0:T(8,128)(2,1)}, bf16[1,1024,128]{2,1,0:T(8,128...) custom-call(bf16[128,2048]{1,0:T(8,128)(2,1)} %refs_0_.1, ...), custom_call_target="tpu_custom_call" | custom-call | tf_op jit(solution)/shard_map/gather/pallas_call | solution.py:333
  46.3 0.9 constant_dynamic-slice_fusion
  47.2 0.0 copy-start
  47.2 1.0 copy.16.gq
  48.3 1.0 multiply_exponential_fusion.qdec
  49.3 0.7 compare_select_fusion.within
  50.0 0.7 multiply_exponential_fusion.1.kdec
  50.6 0.0 copy-done.1
  50.6 0.7 broadcast_in_dim.4.bdec
  51.3 0.0 copy-done
  51.3 75.2 %mixer.1 = bf16[128,2048]{1,0:T(8,128)(2,1)} custom-call(bf16[1,1024,256]{2,1,0:T(8,128)(2,1)} %get-tuple-element.12.rq, bf16[1,1024,256]{2,1,0:T(8,128)(2,1)} %get-tuple-element.13.rk, bf16[1,1024,256]{2,1,0:T(8,128)(2,1)} %get-tuple-element.14.rv, bf16[1,1024,128]{2,1,0:T(8,128)(2,1)} %get-tuple-element.15.fq, ...), custom_call_target="tpu_custom_call" | custom-call | tf_op jit(solution)/shard_map/mixer/pallas_call | solution.py:747
  126.5 1.9 %copy.18 = bf16[128,2048]{1,0:T(8,128)(2,1)} copy(bf16[128,2048]{1,0:T(8,128)(2,1)} %mixer.1) | data formatting | bytes 1048576
  (4 shorter events, 0.0 us)
Async XLA Ops:
  3.1 47.5 %copy-start.1 = (f32[2]{0:T(128)S(1)}, f32[2]{0:T(128)}, u32[]{:S(2)}) copy-start(f32[2]{0:T(128)} %constant.66.clone) | copy-start | bytes 28
  47.2 4.1 %copy-start = (f32[16,1,256]{2,1,0:T(1,128)}, f32[16,1,256]{2,1,0:T(1,128)S(1)}, u32[]{:S(2)}) copy-start(f32[16,1,256]{2,1,0:T(1,128)S(1)} %constant_dynamic-slice_fusion) | copy-start | bytes 49156
